TPU v7x, 32 devices: a whole 2x2x4 slice. The times are simulated.
32 devices in a mesh: sp: 16 (over z, y, x), tp: 2 (over core).
Axes of the slice: x: 2, y: 2, z: 4, core: 2. Of those that a mesh axis runs over, the one named last changes fastest.
Arguments:
- residual: bfloat16 [4096, 2048], P(('sp', 'tp')), may hold values from -6 to 6
- query_nope: bfloat16 [4096, 1024], P('sp', 'tp'), may hold values from -24 to 24
- query_rope: bfloat16 [4096, 512], P('sp', 'tp'), may hold values from -400 to 400
- latent: bfloat16 [4096, 256], P(('sp', 'tp')), may hold values from -6 to 6
- key_rope: bfloat16 [4096, 64], P(('sp', 'tp')), may hold values from -6 to 6
- key_up: bfloat16 [256, 1024], P(None, 'tp'), may hold values from -0.375 to 0.375
- value_up: bfloat16 [256, 1024], P(None, 'tp'), may hold values from -0.375 to 0.375
- out_proj: bfloat16 [1024, 2048], replicated, may hold values from -0.375 to 0.375
- norm_gain: float32 [2048], replicated, may hold values from 0.1 to 1.9
- routes: int32 [4096, 2], P(('sp', 'tp')), may hold values from 0 to 15, all different within a row; in each aligned block of 128 rows (0 to 127, 128 to 255, ...) at most 32 rows name the same one
- route_weight: float32 [4096, 2], P(('sp', 'tp')), may hold values from 0.3 to 2.5
- w_gate: bfloat16 [16, 2048, 512], P('sp', None, 'tp'), may hold values from -0.125 to 0.125
- w_up: bfloat16 [16, 2048, 512], P('sp', None, 'tp'), may hold values from -0.125 to 0.125
- w_down: bfloat16 [16, 512, 2048], P('sp', 'tp'), may hold values from -0.25 to 0.25
Outputs:
- mixed: bfloat16 [4096, 2048], P(('sp', 'tp'))
Inputs may be any that keep to these rules, and one draw needn't show every extreme that they name: `routes`: each row names 2 different experts. Among the rows of one device no expert is named more than 32 times, a bound that some block reaches by the rows of some device.
All inputs are finite; a program needn't handle non-finite values.
Results may differ from a plain program's by a relative error of at most 0.015.
Values may be sent and summed in bfloat16 or wider, within the bound.
A program may use at most 128 MiB of HBM per device.

v0:
```python
import jax
import jax.numpy as jnp
from jax import lax
from jax.sharding import PartitionSpec as P

QK_NOPE = 128
QK_ROPE = 64
V_DIM = 128
SEGMENT = 64


EPSILON = 1e-06
ROPE_BASE = 10000.0
NEG_LARGE = -1e30


def rotary(values, positions):
    half_width = values.shape[-1] // 2
    inverse = ROPE_BASE ** (-2.0 * jnp.arange(half_width, dtype=jnp.float32) / values.shape[-1])
    angles = positions.astype(jnp.float32)[:, None] * inverse[None, :]
    cosine = jnp.cos(angles)
    sine_part = jnp.sin(angles)
    if values.ndim == 3:
        cosine = cosine[:, None, :]
        sine_part = sine_part[:, None, :]
    first_half = values[..., :half_width]
    second = values[..., half_width:]
    return jnp.concatenate(
        [first_half * cosine - second * sine_part, second * cosine + first_half * sine_part],
        axis=-1,
    )


def local(
    residual,
    query_nope,
    query_rope,
    latent,
    key_rope,
    key_up,
    value_up,
    out_proj,
    norm_gain,
    routes,
    route_weight,
    w_gate,
    w_up,
    w_down,
):
    tp_count = lax.axis_size("tp")
    tp_index = lax.axis_index("tp")
    sp_index = lax.axis_index("sp")
    row_count = residual.shape[0]
    tok_dev = query_nope.shape[0]
    heads_here = query_nope.shape[1] // QK_NOPE
    score_scale = (QK_NOPE + QK_ROPE) ** (-0.5)
    query_first = sp_index * tok_dev
    query_pos = query_first + jnp.arange(tok_dev, dtype=jnp.int32)
    query_rot = rotary(
        query_rope.astype(jnp.float32).reshape(tok_dev, heads_here, QK_ROPE), query_pos
    ).astype(jnp.bfloat16)
    query_heads = query_nope.reshape(tok_dev, heads_here, QK_NOPE)
    key_pos = query_first + tp_index * row_count + jnp.arange(row_count, dtype=jnp.int32)
    key_rot = rotary(key_rope.astype(jnp.float32), key_pos).astype(jnp.bfloat16)
    query_segment = query_pos // SEGMENT
    last_segment = (query_first + tok_dev - 1) // SEGMENT
    initial = (
        jnp.full((heads_here, tok_dev), NEG_LARGE, jnp.float32),
        jnp.zeros((heads_here, tok_dev), jnp.float32),
        jnp.zeros((tok_dev, heads_here, V_DIM), jnp.float32),
    )
    paired = (
        lax.all_gather(latent, "tp", axis=0, tiled=True),
        lax.all_gather(key_rot, "tp", axis=0, tiled=True),
    )
    lat_rows = lax.all_gather(paired[0], "sp", axis=0, tiled=True)
    rot_rows = lax.all_gather(paired[1], "sp", axis=0, tiled=True)
    piece_rows = lat_rows.shape[0]
    key_block = piece_rows
    while key_block > 2048 and key_block % 2 == 0:
        key_block //= 2
    block_count = piece_rows // key_block

    def one_block(state_now, inputs):
        lat_block, rot_block, offset = inputs
        key_nope = jnp.dot(lat_block, key_up, preferred_element_type=jnp.float32).astype(
            jnp.bfloat16
        )
        key_nope = key_nope.reshape(key_block, heads_here, QK_NOPE)
        value_rows = jnp.dot(lat_block, value_up, preferred_element_type=jnp.float32).astype(
            jnp.bfloat16
        )
        value_rows = value_rows.reshape(key_block, heads_here, V_DIM)
        scores = jnp.einsum(
            "qhd,khd->hqk", query_heads, key_nope, preferred_element_type=jnp.float32
        )
        scores = (
            scores
            + jnp.einsum("qhr,kr->hqk", query_rot, rot_block, preferred_element_type=jnp.float32)
        ) * score_scale
        key_segment = (offset + jnp.arange(key_block, dtype=jnp.int32)) // SEGMENT
        allowed = (key_segment[None, :] <= query_segment[:, None])[None]
        scores = jnp.where(allowed, scores, NEG_LARGE)
        old_max, old_sum, old_acc = state_now
        new_max = jnp.maximum(old_max, jnp.max(scores, axis=-1))
        weights = jnp.where(allowed, jnp.exp(scores - new_max[:, :, None]), 0.0)
        shrink = jnp.exp(old_max - new_max)
        new_sum = old_sum * shrink + jnp.sum(weights, axis=-1)
        new_acc = old_acc * shrink.T[:, :, None] + jnp.einsum(
            "hqk,khv->qhv",
            weights.astype(jnp.bfloat16),
            value_rows,
            preferred_element_type=jnp.float32,
        )
        return ((new_max, new_sum, new_acc), None)

    def compute(state_now):
        result, unused = lax.scan(
            one_block,
            state_now,
            (
                lat_rows.reshape(block_count, key_block, lat_rows.shape[1]),
                rot_rows.reshape(block_count, key_block, rot_rows.shape[1]),
                jnp.arange(block_count, dtype=jnp.int32) * key_block,
            ),
        )
        return result

    def keep_state(state_now):
        return state_now

    row_max, weight_sum, weighted = lax.cond(
        jnp.int32(0) // SEGMENT <= last_segment, compute, keep_state, initial
    )
    attn_out = (
        (weighted / weight_sum.T[:, :, None])
        .astype(jnp.bfloat16)
        .reshape(tok_dev, heads_here * V_DIM)
    )
    all_heads = lax.all_to_all(attn_out, "tp", split_axis=0, concat_axis=1, tiled=True)
    projected = jnp.dot(all_heads, out_proj, preferred_element_type=jnp.float32)
    hidden_wide = residual.astype(jnp.float32) + projected
    hidden = hidden_wide.astype(jnp.bfloat16)
    hidden_wide = hidden.astype(jnp.float32)
    normed = hidden_wide * lax.rsqrt(
        jnp.mean(hidden_wide * hidden_wide, axis=-1, keepdims=True) + EPSILON
    )
    normed = (normed * norm_gain[None, :]).astype(jnp.bfloat16)
    expert_count = lax.axis_size("sp")
    capacity = max(2, 2 * (row_count * tp_count) // expert_count)
    top_count = routes.shape[1]
    width = normed.shape[1]
    flat_expert = routes.reshape(-1)
    onehot = (flat_expert[:, None] == jnp.arange(expert_count, dtype=jnp.int32)[None, :]).astype(
        jnp.int32
    )
    slot_rank = jnp.sum(jnp.cumsum(onehot, axis=0) * onehot, axis=1) - 1
    slot_index = flat_expert * capacity + slot_rank
    outgoing = (
        jnp.zeros((expert_count * capacity, width), jnp.bfloat16)
        .at[slot_index]
        .set(jnp.repeat(normed, top_count, axis=0))
    )
    gate_weight = w_gate[0]
    up_weight = w_up[0]
    down_weight = w_down[0]
    shard_piece = lax.all_gather(
        lax.all_to_all(
            outgoing.reshape(expert_count, capacity, width),
            "sp",
            split_axis=0,
            concat_axis=0,
            tiled=True,
        ),
        "tp",
        axis=0,
        tiled=True,
    )
    gate_part = jnp.dot(shard_piece, gate_weight, preferred_element_type=jnp.float32)
    up_part = jnp.dot(shard_piece, up_weight, preferred_element_type=jnp.float32)
    activated = (jax.nn.silu(gate_part) * up_part).astype(jnp.bfloat16)
    product = jnp.dot(activated, down_weight, preferred_element_type=jnp.float32)
    summed = lax.psum_scatter(
        lax.optimization_barrier(product.astype(jnp.bfloat16))
        .astype(jnp.float32)
        .astype(jnp.bfloat16),
        "tp",
        scatter_dimension=0,
        tiled=True,
    )
    back_rows = lax.all_to_all(summed, "sp", split_axis=0, concat_axis=0, tiled=True)
    picked = back_rows.reshape(expert_count * capacity, width)[slot_index]
    combined = jnp.sum(
        picked.astype(jnp.float32).reshape(row_count, top_count, width) * route_weight[:, :, None],
        axis=1,
    )
    return (hidden_wide + combined).astype(jnp.bfloat16)


def solution(mesh):
    return jax.shard_map(
        local,
        mesh=mesh,
        in_specs=(
            P(("sp", "tp"), None),
            P("sp", "tp"),
            P("sp", "tp"),
            P(("sp", "tp"), None),
            P(("sp", "tp"), None),
            P(None, "tp"),
            P(None, "tp"),
            P(),
            P(),
            P(("sp", "tp"), None),
            P(("sp", "tp"), None),
            P("sp", None, "tp"),
            P("sp", None, "tp"),
            P("sp", "tp", None),
        ),
        out_specs=P(("sp", "tp"), None),
        check_vma=False,
    )
```

profile of v0, /device:TPU:16, one launch (start us, length us, event | category | flops | bytes accessed | tf_op | source)
XLA Modules:
  0.0 297.5 jit_solution(12448938111200499188)
XLA Ops:
  6.5 3.5 %all_gather.15 = bf16[256,256]{1,0:T(8,128)(2,1)} all-gather(bf16[128,256]{1,0:T(8,128)(2,1)} %param.21), channel_id=1, replica_groups=mesh['sp'=16,'tp'=2] {'tp'}, dimensions={0}, use_global_device_ids=true | all-gather | bytes 196608 | tf_op jit(solution)/shard_map/all_gather | solution.py:73
  10.1 0.8 copy.59
  10.9 0.1 eq.29
  11.0 0.1 eq.25
  11.2 1.0 copy.54
  12.2 0.7 convert_element_type.81
  12.9 0.6 reduce-window.6
  13.5 0.2 slice_reduce_fusion
  13.7 0.7 broadcast_multiply_fusion
  14.4 0.1 copy.58
  14.5 0.1 mul.185
  14.7 0.1 fusion.51
  14.9 1.9 all_gather.17
  16.7 0.1 fusion.55
  16.8 0.2 multiply_cosine_fusion
  17.1 36.0 %all_gather.18 = bf16[4096,64]{0,1:T(8,128)(2,1)S(1)} all-gather(bf16[256,64]{0,1:T(8,128)(2,1)S(1)} %all_gather.17), channel_id=1, replica_groups=mesh['sp'=16,'tp'=2] {'sp'}, dimensions={0}, use_global_device_ids=true | all-gather | bytes 557056 | tf_op jit(solution)/shard_map/all_gather | solution.py:77
  53.2 19.3 %all-gather.3.cloned.1.call-done = bf16[4096,256]{1,0:T(8,128)(2,1)} async-done(((bf16[256,256]{1,0:T(8,128)(2,1)}), bf16[4096,256]{1,0:T(8,128)(2,1)}) %all-gather.3.cloned.1.call-update) | async-done | bytes 2097168 | tf_op jit(solution)/shard_map/all_gather | solution.py:76
  72.5 43.9 %conditional.1 = (f32[4,256]{1,0:T(4,128)}, f32[256,4,128]{0,2,1:T(8,128)}) conditional(s32[]{:T(128)} %convert_element_type.80, () %tuple.28, (bf16[4096,256]{1,0:T(8,128)(2,1)}, bf16[4096,64]{0,1:T(8,128)(2,1)S(1)}, bf16[256,512]{1,0:T(8,128)(2,1)}, s32[256]{0:T(256)S(1)}, s32[256]{0:T(256)S(1)}, /*index=5*/s32[]{:T(128)}, ...), branch_computations={%region_0.1_spmd, %region_1.6_spmd.clone} | conditional | flops 2439948032 | bytes 85153152 | solution.py:132
  72.5 1.1 copy.55
  73.6 0.2 copy.52
  73.8 42.6 %while.20 = (s32[]{:T(128)}, f32[4,256]{1,0:T(4,128)S(1)}, f32[4,256]{1,0:T(4,128)}, f32[256,4,128]{0,2,1:T(8,128)}, s32[2]{0:T(128)S(1)}, /*index=5*/s32[256]{0...) while((s32[]{:T(128)}, f32[4,256]{1,0:T(4,128)S(1)}, ...), condition=%wide.region_5.5_spmd.clone, body=%wide.region_2.4_spmd.clone.sunk | while | flops 2439944192 | bytes 83052784 | solution.py:118
  73.8 2.0 convolution_convert_fusion.5
  75.9 1.3 fusion.95
  77.2 0.7 dynamic_slice.45
  77.8 0.6 add_select_fusion.2
  78.5 0.5 broadcast_compare_fusion.2
  78.9 5.5 %fusion.96 = (f32[4,256]{1,0:T(4,128)S(1)}, f32[4,256,2048]{1,2,0:T(8,128)}) fusion(bf16[256,4,64]{0,2,1:T(8,128)(2,1)S(1)} %get-tuple-element.537, bf16[2,2048,64]{1,2,0:T(8,128)(2,1)S(1)} %get-tuple-element.536, s32[]{:T(128)} %get-tuple-element.513, f32[4,2048,256]{2,1,0:T(8,128)S(1)} %fusion.95, pred[256,2048]{0,1:T(8,128)(4,1)S(1)} %broadcast_compare_fusion.2), kind=kOutput, calls=%fused_computation.105.clone.1 | convolution fusion | flops 276823040 | bytes 17698820 | tf_op jit(solution)/shard_map/cond/branch_1_fun/while/body/eval_jaxpr/qhr,kr->hqk/dot_general | solution.py:99
  84.5 2.1 convolution_convert_fusion.6
  86.6 6.0 %fusion.100 = f32[256,4,128]{0,2,1:T(8,128)} fusion(bf16[2048,4,128]{0,2,1:T(8,128)(2,1)S(1)} %bitcast.115, f32[4,256,2048]{1,2,0:T(8,128)} %get-tuple-element.497, f32[4,256]{1,0:T(4,128)S(1)} %get-tuple-element.528, pred[256,2048]{0,1:T(8,128)(4,1)S(1)} %broadcast_compare_fusion.2, f32[256,4,128]{0,2,1:T(8,128)} %get-tuple-element.516, ...), kind=kOutput, calls=%fused_computation.15.clone.1 | convolution fusion | flops 543555584 | bytes 12066817 | tf_op jit(solution)/shard_map/cond/branch_1_fun/while/body/eval_jaxpr/hqk,khv->qhv/dot_general | solution.py:109
  92.6 1.5 fusion.98
  94.1 0.6 fusion.99
  94.8 2.0 convolution_convert_fusion.5
  96.8 1.3 fusion.95
  98.1 0.7 dynamic_slice.45
  98.7 0.6 add_select_fusion.2
  99.4 0.5 broadcast_compare_fusion.2
  99.9 5.5 %fusion.96 = (f32[4,256]{1,0:T(4,128)S(1)}, f32[4,256,2048]{1,2,0:T(8,128)}) fusion(bf16[256,4,64]{0,2,1:T(8,128)(2,1)S(1)} %get-tuple-element.537, bf16[2,2048,64]{1,2,0:T(8,128)(2,1)S(1)} %get-tuple-element.536, s32[]{:T(128)} %get-tuple-element.513, f32[4,2048,256]{2,1,0:T(8,128)S(1)} %fusion.95, pred[256,2048]{0,1:T(8,128)(4,1)S(1)} %broadcast_compare_fusion.2), kind=kOutput, calls=%fused_computation.105.clone.1 | convolution fusion | flops 276823040 | bytes 17698820 | tf_op jit(solution)/shard_map/cond/branch_1_fun/while/body/eval_jaxpr/qhr,kr->hqk/dot_general | solution.py:99
  105.4 2.1 convolution_convert_fusion.6
  107.5 6.1 %fusion.100 = f32[256,4,128]{0,2,1:T(8,128)} fusion(bf16[2048,4,128]{0,2,1:T(8,128)(2,1)S(1)} %bitcast.115, f32[4,256,2048]{1,2,0:T(8,128)} %get-tuple-element.497, f32[4,256]{1,0:T(4,128)S(1)} %get-tuple-element.528, pred[256,2048]{0,1:T(8,128)(4,1)S(1)} %broadcast_compare_fusion.2, f32[256,4,128]{0,2,1:T(8,128)} %get-tuple-element.516, ...), kind=kOutput, calls=%fused_computation.15.clone.1 | convolution fusion | flops 543555584 | bytes 12066817 | tf_op jit(solution)/shard_map/cond/branch_1_fun/while/body/eval_jaxpr/hqk,khv->qhv/dot_general | solution.py:109
  113.6 1.5 fusion.98
  115.1 1.3 fusion.99
  116.4 1.1 divide_convert_fusion
  117.5 0.1 reshape.255
  117.6 0.2 copy.65
  117.8 3.9 %all_to_all.29 = bf16[2,128,512]{2,1,0:T(8,128)(2,1)S(1)} all-to-all(bf16[2,128,512]{2,1,0:T(8,128)(2,1)S(1)} %copy.65), channel_id=1, replica_groups=mesh['sp'=16,'tp'=2] {'tp'}, dimensions={0} | all-to-all | bytes 524288 | tf_op jit(solution)/shard_map/all_to_all | solution.py:140
  121.7 0.2 copy.57
  121.9 3.1 %multiply_reduce_fusion.1 = (f32[128]{0:T(128)S(1)}, f32[128,2048]{1,0:T(8,128)S(1)}) fusion(bf16[128,1024]{0,1:T(8,128)(2,1)S(1)} %bitcast.120, bf16[1024,2048]{1,0:T(8,128)(2,1)} %param.25, bf16[128,2048]{1,0:T(8,128)(2,1)} %param.18), kind=kOutput, calls=%fused_computation.66 | convolution fusion | flops 538443648 | bytes 6029824 | tf_op jit(solution)/shard_map/dot_general | solution.py:141
  125.0 1.0 copy-done.1
  126.1 0.2 multiply_convert_fusion
  126.2 0.6 broadcast_in_dim.71
  126.9 1.2 reshape.245
  128.1 3.5 %scatter_custom_fusion = bf16[512,2048]{1,0:T(8,128)(2,1)S(1)} fusion(s32[256]{0:T(256)S(1)} %bitcast.123, bf16[256,2048]{1,0:T(8,128)(2,1)} %reshape.245, bf16[]{:T(256)} %constant.158.clone.1), kind=kCustom, calls=%fused_computation.67 | custom fusion | bytes 2097664 | tf_op jit(solution)/shard_map/scatter | solution.py:162
  131.6 52.6 %all_to_all.30 = bf16[16,32,2048]{2,1,0:T(8,128)(2,1)} all-to-all(bf16[16,32,2048]{2,1,0:T(8,128)(2,1)S(1)} %bitcast.116), channel_id=1, replica_groups=mesh['sp'=16,'tp'=2] {'sp'}, dimensions={0} | all-to-all | bytes 4194304 | tf_op jit(solution)/shard_map/all_to_all | solution.py:168
  184.3 14.0 %all-gather.5.cloned.1.call-done = bf16[32,32,2048]{2,1,0:T(8,128)(2,1)} async-done(((bf16[16,32,2048]{2,1,0:T(8,128)(2,1)}), bf16[32,32,2048]{2,1,0:T(8,128)(2,1)}) %all-gather.5.cloned.1.call-update) | async-done | bytes 4194320 | tf_op jit(solution)/shard_map/all_gather | solution.py:167
  198.3 3.7 %fusion.36 = f32[32,32,256]{2,1,0:T(8,128)S(1)} fusion(bf16[32,32,2048]{2,1,0:T(8,128)(2,1)} %all-gather.5.cloned.1.call-done, bf16[1,2048,256]{2,1,0:T(8,128)(2,1)} %param.29), kind=kOutput, calls=%fused_computation.57 | convolution fusion | flops 1073741824 | bytes 6291456 | tf_op jit(solution)/shard_map/dot_general | solution.py:179
  202.0 8.5 %convolution_convert_fusion.2 = bf16[32,32,2048]{2,1,0:T(8,128)(2,1)} fusion(bf16[32,32,2048]{2,1,0:T(8,128)(2,1)} %all-gather.5.cloned.1.call-done, bf16[1,256,2048]{2,1,0:T(8,128)(2,1)S(1)} %copy-done, bf16[1,2048,256]{2,1,0:T(8,128)(2,1)S(1)} %copy-done.6, f32[32,32,256]{2,1,0:T(8,128)S(1)} %fusion.36), kind=kOutput, calls=%fused_computation.48 | convolution fusion | flops 2151153664 | bytes 11534336 | tf_op jit(solution)/shard_map/dot_general | solution.py:182
  210.5 13.5 %reduce-scatter.2.cloned.1.call-done = bf16[16,32,2048]{2,1,0:T(8,128)(2,1)} async-done(((bf16[32,32,2048]{2,1,0:T(8,128)(2,1)}), bf16[16,32,2048]{2,1,0:T(8,128)(2,1)}) %reduce-scatter.2.cloned.1.call-update) | async-done | bytes 2097168 | tf_op jit(solution)/shard_map/reduce_scatter | solution.py:183
  224.0 7.0 %all-to-all-start.2 = ((bf16[16,32,2048]{2,1,0:T(8,128)(2,1)}), bf16[16,32,2048]{2,1,0:T(8,128)(2,1)S(1)}, u32[]{:S(2)}, u32[]{:S(2)}) async-start(bf16[16,32,2048]{2,1,0:T(8,128)(2,1)} %reduce-scatter.2.cloned.1.call-done), calls=%async_computation.3 | async-start | bytes 4194304 | tf_op jit(solution)/shard_map/all_to_all | solution.py:191
  231.0 0.1 copy.62
  231.1 48.3 %all-to-all-done.2 = bf16[16,32,2048]{2,1,0:T(8,128)(2,1)S(1)} async-done(((bf16[16,32,2048]{2,1,0:T(8,128)(2,1)}), bf16[16,32,2048]{2,1,0:T(8,128)(2,1)S(1)}, u32[]{:S(2)}, u32[]{:S(2)}) %all-to-all-start.2) | async-done | bytes 2097184 | tf_op jit(solution)/shard_map/all_to_all | solution.py:191
  279.4 2.4 gather_fusion
  281.8 3.5 %reshape.232 = f32[128,2,2048]{2,1,0:T(2,128)} reshape(bf16[256,2048]{1,0:T(8,128)(2,1)} %gather_fusion) | data formatting | bytes 3145728 | tf_op jit(solution)/shard_map/convert_element_type | solution.py:194
  285.2 4.8 %multiply_reduce_fusion = f32[128,2048]{1,0:T(8,128)S(1)} fusion(f32[128,2,2048]{2,1,0:T(2,128)} %reshape.232, f32[128,2]{1,0:T(8,128)S(1)} %copy.62), kind=kLoop, calls=%fused_computation.52 | loop fusion | flops 786432 | bytes 3146752 | tf_op jit(solution)/shard_map/reduce_sum | solution.py:193
  290.1 0.9 add_convert_fusion
  (55 shorter events, 0.4 us)
Async XLA Ops:
  6.5 195.5 %copy-start = (bf16[1,256,2048]{2,1,0:T(8,128)(2,1)S(1)}, bf16[1,256,2048]{2,1,0:T(8,128)(2,1)}, u32[]{:S(2)}) copy-start(bf16[1,256,2048]{2,1,0:T(8,128)(2,1)} %param.31) | copy-start | bytes 3145732
  6.5 65.9 %all-gather.3.cloned.1.call-start = ((), (), s32[]{:S(2)}) async-start(), calls=%async_computation.4 | async-start | bytes 2228224 | tf_op jit(solution)/shard_map/all_gather | solution.py:76
  10.0 188.2 %all-gather.5.cloned.1.call-start = ((), (), s32[]{:S(2)}) async-start(), calls=%async_computation.5 | async-start | bytes 6291456 | tf_op jit(solution)/shard_map/all_gather | solution.py:167
  78.9 5.5 %copy-start.3 = (bf16[256,512]{1,0:T(8,128)(2,1)S(1)}, bf16[256,512]{1,0:T(8,128)(2,1)}, u32[]{:S(2)}) copy-start(bf16[256,512]{1,0:T(8,128)(2,1)} %get-tuple-element.538) | copy-start | bytes 786436 | tf_op jit(solution)/shard_map/cond/branch_1_fun/while
  84.5 8.2 %slice-start = ((s8[8388608]{0:T(1024)(128)(4,1)}), s8[4194304]{0:T(1024)(128)(4,1)S(1)}, s32[]{:S(2)}) async-start(s8[8388608]{0:T(1024)(128)(4,1)} %bitcast.110), calls=%async_computation.7 | async-start | bytes 8388608 | tf_op jit(solution)/shard_map/cond/branch_1_fun/while
  86.6 6.0 %slice-start.1 = ((s8[8388608]{0:T(1024)(128)(4,1)}), s8[4194304]{0:T(1024)(128)(4,1)S(1)}, s32[]{:S(2)}) async-start(s8[8388608]{0:T(1024)(128)(4,1)} %bitcast.110), calls=%async_computation.8 | async-start | bytes 8388608 | tf_op jit(solution)/shard_map/cond/branch_1_fun/while
  99.9 5.5 %copy-start.3 = (bf16[256,512]{1,0:T(8,128)(2,1)S(1)}, bf16[256,512]{1,0:T(8,128)(2,1)}, u32[]{:S(2)}) copy-start(bf16[256,512]{1,0:T(8,128)(2,1)} %get-tuple-element.538) | copy-start | bytes 786436 | tf_op jit(solution)/shard_map/cond/branch_1_fun/while
  105.4 8.2 %slice-start = ((s8[8388608]{0:T(1024)(128)(4,1)}), s8[4194304]{0:T(1024)(128)(4,1)S(1)}, s32[]{:S(2)}) async-start(s8[8388608]{0:T(1024)(128)(4,1)} %bitcast.110), calls=%async_computation.7 | async-start | bytes 8388608 | tf_op jit(solution)/shard_map/cond/branch_1_fun/while
  107.5 6.1 %slice-start.1 = ((s8[8388608]{0:T(1024)(128)(4,1)}), s8[4194304]{0:T(1024)(128)(4,1)S(1)}, s32[]{:S(2)}) async-start(s8[8388608]{0:T(1024)(128)(4,1)} %bitcast.110), calls=%async_computation.8 | async-start | bytes 8388608 | tf_op jit(solution)/shard_map/cond/branch_1_fun/while
  117.5 8.6 %copy-start.4 = (f32[2048]{0:T(1024)S(1)}, f32[2048]{0:T(1024)}, u32[]{:S(2)}) copy-start(f32[2048]{0:T(1024)} %param.26) | copy-start | bytes 24580
  125.0 1.1 copy-start.1
  184.2 17.8 %copy-start.6 = (bf16[1,2048,256]{2,1,0:T(8,128)(2,1)S(1)}, bf16[1,2048,256]{2,1,0:T(8,128)(2,1)}, u32[]{:S(2)}) copy-start(bf16[1,2048,256]{2,1,0:T(8,128)(2,1)} %param.30) | copy-start | bytes 3145732
  184.2 39.8 %reduce-scatter.2.cloned.1.call-start = ((), (), s32[]{:S(2)}) async-start(), calls=%async_computation.6 | async-start | bytes 6291456 | tf_op jit(solution)/shard_map/reduce_scatter | solution.py:183
  210.5 20.5 %copy-start.5 = (f32[128,2]{0,1:T(2,128)S(1)}, f32[128,2]{0,1:T(2,128)}, u32[]{:S(2)}) copy-start(f32[128,2]{0,1:T(2,128)} %param.28) | copy-start | bytes 3076
  224.0 55.4 %all-to-all-start.2 = ((bf16[16,32,2048]{2,1,0:T(8,128)(2,1)}), bf16[16,32,2048]{2,1,0:T(8,128)(2,1)S(1)}, u32[]{:S(2)}, u32[]{:S(2)}) async-start(bf16[16,32,2048]{2,1,0:T(8,128)(2,1)} %reduce-scatter.2.cloned.1.call-done), calls=%async_computation.3 | async-start | bytes 4194304 | tf_op jit(solution)/shard_map/all_to_all | solution.py:191
  281.8 8.3 %copy-start.2 = (f32[128,2048]{1,0:T(8,128)S(1)}, f32[128,2048]{1,0:T(8,128)}, u32[]{:S(2)}) copy-start(f32[128,2048]{1,0:T(8,128)} %copy-done.1) | copy-start | bytes 3145732
Sparse Core Ops, SparseCore 0:
  10.2 62.2 all-gather.2
  184.3 13.8 all-gather.4
  210.7 13.3 reduce-scatter.1
where the time goes:
time: 298 us
  blocking collectives  97.9 us (33%)
  waiting for transfers between devices  95.1 us (32%)
  matrix products  49.3 us (17%)
  local copies, waits for them, and re-layouts  17.9 us (6%)
  other arithmetic  16.7 us (6%)
  between operations  13.3 us (4%)
  starting transfers between devices  7.05 us (2%)
    all_to_all x1, blocking collectives, local(): lax.all_to_all(outgoing.reshape(expert_count, capacity, width), 'sp', spl...  52.6 us
    all_to_all x1, waiting for transfers between devices, local(): lax.all_to_all(summed, 'sp', split_axis=0, concat_axis=0, tiled=True)  48.3 us
    all_gather x1, blocking collectives, local(): rot_rows = lax.all_gather(paired[1], 'sp', axis=0, tiled=True)  36 us
    all_gather x1, waiting for transfers between devices, local(): lat_rows = lax.all_gather(paired[0], 'sp', axis=0, tiled=True)  19.3 us
    all_gather x1, waiting for transfers between devices, local(): lax.all_gather(lax.all_to_all(outgoing.reshape(expert_count, capacity, wi...  14 us
    reduce_scatter x1, waiting for transfers between devices, local(): lax.psum_scatter(lax.optimization_barrier(product.astype(jnp.bfloat16)).a...  13.5 us
    dot_general x2, matrix products, one_block(): jnp.einsum('hqk,khv->qhv', weights.astype(jnp.bfloat16), value_rows, pref...  12.1 us
    dot_general x2, matrix products, one_block(): jnp.einsum('qhr,kr->hqk', query_rot, rot_block, preferred_element_type=jn...  11 us
  transfers between devices with their start and end apart: 4, of which 4 were waited for; matrix products, arithmetic and copies ran while one was open for 2% of the time, Pallas kernels for 0%

commit v1 on v0

v1 whole, which is shorter than its diff:
```python
import functools
import math

import jax
import jax.numpy as jnp
from jax import lax
from jax.experimental import pallas as pl
from jax.experimental.pallas import tpu as pltpu
from jax.sharding import PartitionSpec as P

QK_NOPE = 128
QK_ROPE = 64
V_DIM = 128
SEGMENT = 64


EPSILON = 1e-06
ROPE_BASE = 10000.0
NEG_LARGE = -1e30


def rotary(values, positions):
    half_width = values.shape[-1] // 2
    inverse = ROPE_BASE ** (-2.0 * jnp.arange(half_width, dtype=jnp.float32) / values.shape[-1])
    angles = positions.astype(jnp.float32)[:, None] * inverse[None, :]
    cosine = jnp.cos(angles)
    sine_part = jnp.sin(angles)
    if values.ndim == 3:
        cosine = cosine[:, None, :]
        sine_part = sine_part[:, None, :]
    first_half = values[..., :half_width]
    second = values[..., half_width:]
    return jnp.concatenate(
        [first_half * cosine - second * sine_part, second * cosine + first_half * sine_part],
        axis=-1,
    )


MESH = pl.DeviceIdType.MESH
VMEM = pl.BlockSpec(memory_space=pltpu.VMEM)


def greet(peers):
    barrier = pltpu.get_barrier_semaphore()
    for peer in peers:
        pl.semaphore_signal(barrier, inc=1, device_id=peer, device_id_type=MESH)
    pl.semaphore_wait(barrier, len(peers))


def far_first(count):
    return sorted(range(1, count), key=lambda step: abs(2 * step - count))


def send(source, target, send_sem, recv_sem, peer):
    copy = pltpu.make_async_remote_copy(
        src_ref=source,
        dst_ref=target,
        send_sem=send_sem,
        recv_sem=recv_sem,
        device_id=peer,
        device_id_type=MESH,
    )
    copy.start()
    return copy


def arrived(block, semaphore):
    pltpu.make_async_copy(block, block, semaphore).wait()


def gather_kernel(n_sp, n_tp, inner, own_ref, out_ref, send_sem, recv_sem, local_sem):
    sp, tp = lax.axis_index("sp"), lax.axis_index("tp")
    outer = n_sp // inner
    group, member = sp // inner, sp % inner

    def column(step):
        return ((group + step) % outer) * inner + member

    def mate(step):
        return group * inner + (member + step) % inner

    others = [(column(step), tp) for step in far_first(outer)]
    mates = [(mate(step), tp) for step in range(1, inner)]
    twins = [(sp, (tp + step) % n_tp) for step in range(1, n_tp)]
    greet(others + mates + twins)
    copies = []

    def push(source, block, peers):
        for peer in peers:
            copies.append(
                send(
                    source, out_ref.at[block], send_sem.at[len(copies)], recv_sem.at[block], peer
                )
            )

    mine = sp * n_tp + tp
    keep = pltpu.make_async_copy(own_ref, out_ref.at[mine], local_sem)
    keep.start()
    push(own_ref, mine, others + mates + twins)
    for step in sorted(range(1, outer), key=lambda step: min(step, outer - step)):
        block = column(step) * n_tp + tp
        arrived(out_ref.at[block], recv_sem.at[block])
        push(out_ref.at[block], block, mates + twins)
    for step in range(outer):
        for hop in range(1, inner):
            source = ((group + step) % outer) * inner + (member + hop) % inner
            block = source * n_tp + tp
            arrived(out_ref.at[block], recv_sem.at[block])
            push(out_ref.at[block], block, twins)
    for twin in twins:
        for source in range(n_sp):
            block = source * n_tp + twin[1]
            arrived(out_ref.at[block], recv_sem.at[block])
    keep.wait()
    for copy in copies:
        copy.wait_send()


def gather_rows(own, n_sp, n_tp):
    inner = math.gcd(n_sp, 4)
    outer = n_sp // inner
    sends = (outer - 1) + outer * (inner - 1) + n_sp * (n_tp - 1)
    return pl.pallas_call(
        functools.partial(gather_kernel, n_sp, n_tp, inner),
        out_shape=jax.ShapeDtypeStruct((n_sp * n_tp,) + own.shape, own.dtype),
        in_specs=[VMEM],
        out_specs=VMEM,
        scratch_shapes=[
            pltpu.SemaphoreType.DMA((sends,)),
            pltpu.SemaphoreType.DMA((n_sp * n_tp,)),
            pltpu.SemaphoreType.DMA,
        ],
        compiler_params=pltpu.CompilerParams(collective_id=0, has_side_effects=True),
        name="gather_rows",
    )(own)


def dispatch_kernel(n_sp, n_tp, rows_ref, out_ref, send_sem, recv_sem, local_sem):
    sp, tp = lax.axis_index("sp"), lax.axis_index("tp")
    peers = [((sp + step) % n_sp, tp) for step in far_first(n_sp)]
    twins = [(sp, (tp + step) % n_tp) for step in range(1, n_tp)]
    greet(peers + twins)
    copies = []

    def push(source, core, origin, peer):
        copies.append(
            send(
                source,
                out_ref.at[core, origin],
                send_sem.at[len(copies)],
                recv_sem.at[core * n_sp + origin],
                peer,
            )
        )

    keep = pltpu.make_async_copy(rows_ref.at[sp], out_ref.at[tp, sp], local_sem)
    keep.start()
    for peer in peers:
        push(rows_ref.at[peer[0]], tp, sp, peer)
    for twin in twins:
        push(rows_ref.at[sp], tp, sp, twin)
    for step in reversed(far_first(n_sp)):
        origin = (sp + step) % n_sp
        arrived(out_ref.at[tp, origin], recv_sem.at[tp * n_sp + origin])
        for twin in twins:
            push(out_ref.at[tp, origin], tp, origin, twin)
    for twin in twins:
        for origin in range(n_sp):
            arrived(out_ref.at[twin[1], origin], recv_sem.at[twin[1] * n_sp + origin])
    keep.wait()
    for copy in copies:
        copy.wait_send()


def dispatch_rows(rows, n_sp, n_tp):
    sends = n_sp - 1 + n_sp * (n_tp - 1)
    return pl.pallas_call(
        functools.partial(dispatch_kernel, n_sp, n_tp),
        out_shape=jax.ShapeDtypeStruct((n_tp,) + rows.shape, rows.dtype),
        in_specs=[VMEM],
        out_specs=VMEM,
        scratch_shapes=[
            pltpu.SemaphoreType.DMA((sends,)),
            pltpu.SemaphoreType.DMA((n_sp * n_tp,)),
            pltpu.SemaphoreType.DMA,
        ],
        compiler_params=pltpu.CompilerParams(collective_id=1, has_side_effects=True),
        name="dispatch_rows",
    )(rows)


def return_kernel(
    n_sp, n_tp, part_ref, out_ref, half_ref, sum_ref, twin_send, twin_recv, send_sem, recv_sem, local_sem
):
    sp, tp = lax.axis_index("sp"), lax.axis_index("tp")
    order = far_first(n_sp)
    peers = [((sp + step) % n_sp, tp) for step in order]
    twins = [(sp, (tp + step) % n_tp) for step in range(1, n_tp)]
    greet(peers + twins)
    copies = []
    for target in [peer[0] for peer in peers] + [sp]:
        for step, twin in enumerate(twins):
            slot = step * n_sp + target
            copies.append(
                send(
                    part_ref.at[twin[1], target],
                    half_ref.at[step, target],
                    twin_send.at[slot],
                    twin_recv.at[slot],
                    twin,
                )
            )

    def total(target):
        value = part_ref[tp, target].astype(jnp.float32)
        for step in range(n_tp - 1):
            arrived(half_ref.at[step, target], twin_recv.at[step * n_sp + target])
            value = value + half_ref[step, target].astype(jnp.float32)
        sum_ref[target] = value.astype(sum_ref.dtype)

    for number, peer in enumerate(peers):
        total(peer[0])
        copies.append(
            send(sum_ref.at[peer[0]], out_ref.at[sp], send_sem.at[number], recv_sem.at[sp], peer)
        )
    total(sp)
    keep = pltpu.make_async_copy(sum_ref.at[sp], out_ref.at[sp], local_sem)
    keep.start()
    for step in reversed(order):
        origin = (sp + step) % n_sp
        arrived(out_ref.at[origin], recv_sem.at[origin])
    keep.wait()
    for copy in copies:
        copy.wait_send()


def return_rows(parts, n_sp, n_tp):
    shape = parts.shape[1:]
    return pl.pallas_call(
        functools.partial(return_kernel, n_sp, n_tp),
        out_shape=jax.ShapeDtypeStruct(shape, parts.dtype),
        in_specs=[VMEM],
        out_specs=VMEM,
        scratch_shapes=[
            pltpu.VMEM((n_tp - 1,) + shape, parts.dtype),
            pltpu.VMEM(shape, parts.dtype),
            pltpu.SemaphoreType.DMA(((n_tp - 1) * n_sp,)),
            pltpu.SemaphoreType.DMA(((n_tp - 1) * n_sp,)),
            pltpu.SemaphoreType.DMA((n_sp - 1,)),
            pltpu.SemaphoreType.DMA((n_sp,)),
            pltpu.SemaphoreType.DMA,
        ],
        compiler_params=pltpu.CompilerParams(collective_id=2, has_side_effects=True),
        name="return_rows",
    )(parts)


NT = (((1,), (1,)), ((), ()))


def attention_kernel(
    key_block, latent_width, heads, base_ref, query_ref, kv_ref, key_up_ref, value_up_ref, out_ref, max_ref, sum_ref, acc_ref
):
    first = base_ref[0]
    queries = query_ref.shape[2]
    scale = (QK_NOPE + QK_ROPE) ** (-0.5) * math.log2(math.e)
    max_ref[...] = jnp.full_like(max_ref, NEG_LARGE)
    sum_ref[...] = jnp.zeros_like(sum_ref)
    acc_ref[...] = jnp.zeros_like(acc_ref)

    def block(start, masked):
        start = pl.multiple_of(start, key_block)
        rows = kv_ref[pl.ds(start, key_block), :]
        latent = rows[:, :latent_width]
        rot = rows[:, latent_width:]
        keys = jnp.dot(latent, key_up_ref[...], preferred_element_type=jnp.float32).astype(
            jnp.bfloat16
        )
        values = lax.dot_general(
            value_up_ref[...], latent, NT, preferred_element_type=jnp.float32
        ).astype(jnp.bfloat16)
        if masked:
            key_segment = (
                start + lax.broadcasted_iota(jnp.int32, (key_block, queries), 0)
            ) // SEGMENT
            query_segment = (
                first + lax.broadcasted_iota(jnp.int32, (key_block, queries), 1)
            ) // SEGMENT
            allowed = key_segment <= query_segment
        for head in range(heads):
            wide = jnp.concatenate([keys[:, head * QK_NOPE : (head + 1) * QK_NOPE], rot], axis=1)
            scores = jnp.dot(wide, query_ref[head], preferred_element_type=jnp.float32)
            if masked:
                scores = jnp.where(allowed, scores, NEG_LARGE)
            old_max = max_ref[head]
            new_max = jnp.maximum(old_max, jnp.max(scores, axis=0, keepdims=True))
            weights = jnp.exp2((scores - new_max) * scale)
            shrink = jnp.exp2((old_max - new_max) * scale)
            max_ref[head] = new_max
            sum_ref[head] = sum_ref[head] * shrink + jnp.sum(weights, axis=0, keepdims=True)
            acc_ref[head] = acc_ref[head] * shrink + jnp.dot(
                values[head * V_DIM : (head + 1) * V_DIM],
                weights.astype(jnp.bfloat16),
                preferred_element_type=jnp.float32,
            )

    whole = first // key_block

    def body(step, carry):
        block(step * key_block, False)
        return carry

    lax.fori_loop(0, whole, body, 0)
    block(whole * key_block, True)
    for head in range(heads):
        out_ref[:, head * V_DIM : (head + 1) * V_DIM] = (
            (acc_ref[head] / sum_ref[head]).T.astype(out_ref.dtype)
        )


def attention(base, query, kv, key_up, value_up_t, key_block, latent_width):
    heads, unused, queries = query.shape
    return pl.pallas_call(
        functools.partial(attention_kernel, key_block, latent_width, heads),
        out_shape=jax.ShapeDtypeStruct((queries, heads * V_DIM), jnp.bfloat16),
        in_specs=[pl.BlockSpec(memory_space=pltpu.SMEM), VMEM, VMEM, VMEM, VMEM],
        out_specs=VMEM,
        scratch_shapes=[
            pltpu.VMEM((heads, 1, queries), jnp.float32),
            pltpu.VMEM((heads, 1, queries), jnp.float32),
            pltpu.VMEM((heads, V_DIM, queries), jnp.float32),
        ],
        name="attention",
    )(base, query, kv, key_up, value_up_t)


def local(
    residual,
    query_nope,
    query_rope,
    latent,
    key_rope,
    key_up,
    value_up,
    out_proj,
    norm_gain,
    routes,
    route_weight,
    w_gate,
    w_up,
    w_down,
):
    tp_count = lax.axis_size("tp")
    sp_count = lax.axis_size("sp")
    tp_index = lax.axis_index("tp")
    sp_index = lax.axis_index("sp")
    row_count = residual.shape[0]
    tok_dev = query_nope.shape[0]
    heads_here = query_nope.shape[1] // QK_NOPE
    query_first = sp_index * tok_dev
    query_pos = query_first + jnp.arange(tok_dev, dtype=jnp.int32)
    query_rot = rotary(
        query_rope.astype(jnp.float32).reshape(tok_dev, heads_here, QK_ROPE), query_pos
    ).astype(jnp.bfloat16)
    query_heads = query_nope.reshape(tok_dev, heads_here, QK_NOPE)
    key_pos = query_first + tp_index * row_count + jnp.arange(row_count, dtype=jnp.int32)
    key_rot = rotary(key_rope.astype(jnp.float32), key_pos).astype(jnp.bfloat16)
    width_pad = -(-QK_ROPE // 128) * 128 - QK_ROPE
    packed = jnp.concatenate(
        [latent, key_rot, jnp.zeros((row_count, width_pad), jnp.bfloat16)], axis=1
    )
    gathered = gather_rows(packed, sp_count, tp_count)
    kv_rows = gathered.reshape(sp_count * tok_dev, packed.shape[1])
    query = jnp.concatenate(
        [query_heads, query_rot, jnp.zeros((tok_dev, heads_here, width_pad), jnp.bfloat16)], axis=2
    ).transpose(1, 2, 0)
    key_block = tok_dev * math.gcd(sp_count, 2)
    attn_out = attention(
        query_first.astype(jnp.int32).reshape(1),
        query,
        kv_rows,
        key_up,
        value_up.T,
        key_block,
        latent.shape[1],
    )
    all_heads = lax.all_to_all(attn_out, "tp", split_axis=0, concat_axis=1, tiled=True)
    projected = jnp.dot(all_heads, out_proj, preferred_element_type=jnp.float32)
    hidden_wide = residual.astype(jnp.float32) + projected
    hidden = hidden_wide.astype(jnp.bfloat16)
    hidden_wide = hidden.astype(jnp.float32)
    normed = hidden_wide * lax.rsqrt(
        jnp.mean(hidden_wide * hidden_wide, axis=-1, keepdims=True) + EPSILON
    )
    normed = (normed * norm_gain[None, :]).astype(jnp.bfloat16)
    expert_count = lax.axis_size("sp")
    capacity = max(2, 2 * (row_count * tp_count) // expert_count)
    top_count = routes.shape[1]
    width = normed.shape[1]
    flat_expert = routes.reshape(-1)
    onehot = (flat_expert[:, None] == jnp.arange(expert_count, dtype=jnp.int32)[None, :]).astype(
        jnp.int32
    )
    slot_rank = jnp.sum(jnp.cumsum(onehot, axis=0) * onehot, axis=1) - 1
    slot_index = flat_expert * capacity + slot_rank
    slots = slot_index.reshape(row_count, top_count)
    slot_count = expert_count * capacity
    numbers = jnp.arange(slot_count, dtype=jnp.int32)
    chosen = slots[:, :, None] == numbers[None, None, :]
    place = jnp.any(chosen, axis=1).astype(jnp.bfloat16)
    outgoing = lax.dot_general(
        place, normed, (((0,), (0,)), ((), ())), preferred_element_type=jnp.float32
    ).astype(jnp.bfloat16)
    shares = jnp.sum(jnp.where(chosen, route_weight[:, :, None], 0.0), axis=1)
    share_high = lax.reduce_precision(shares, 8, 7)
    share_low = shares - share_high
    received = dispatch_rows(
        outgoing.reshape(expert_count, capacity, width), sp_count, tp_count
    ).reshape(tp_count * slot_count, width)
    gate_part = jnp.dot(received, w_gate[0], preferred_element_type=jnp.float32)
    up_part = jnp.dot(received, w_up[0], preferred_element_type=jnp.float32)
    activated = (jax.nn.silu(gate_part) * up_part).astype(jnp.bfloat16)
    product = jnp.dot(activated, w_down[0], preferred_element_type=jnp.float32).astype(jnp.bfloat16)
    back_rows = return_rows(
        product.reshape(tp_count, expert_count, capacity, width), sp_count, tp_count
    ).reshape(slot_count, width)
    combined = jnp.dot(
        share_high.astype(jnp.bfloat16), back_rows, preferred_element_type=jnp.float32
    ) + jnp.dot(share_low.astype(jnp.bfloat16), back_rows, preferred_element_type=jnp.float32)
    return (hidden_wide + combined).astype(jnp.bfloat16)


def solution(mesh):
    return jax.shard_map(
        local,
        mesh=mesh,
        in_specs=(
            P(("sp", "tp"), None),
            P("sp", "tp"),
            P("sp", "tp"),
            P(("sp", "tp"), None),
            P(("sp", "tp"), None),
            P(None, "tp"),
            P(None, "tp"),
            P(),
            P(),
            P(("sp", "tp"), None),
            P(("sp", "tp"), None),
            P("sp", None, "tp"),
            P("sp", None, "tp"),
            P("sp", "tp", None),
        ),
        out_specs=P(("sp", "tp"), None),
        check_vma=False,
    )
```

time: 298 us -> 206 us (0.69)
  Pallas kernels: 0 us -> 168 us
  blocking collectives: 97.9 us -> 0 us
  waiting for transfers between devices: 95.1 us -> 1.06 us
  matrix products: 49.3 us -> 22.2 us
  between operations: 13.3 us -> 0.23 us
  other arithmetic: 16.7 us -> 4.1 us
  local copies, waits for them, and re-layouts: 17.9 us -> 6.54 us
  starting transfers between devices: 7.05 us -> 3.62 us
    pallas_call x0 -> x4, Pallas kernels: none -> 168 us  [the longest x1 67.1 us: dispatch_rows(): pl.pallas_call(functools.partial(dispatch_kernel, n_sp, n_tp), out_shape=...]
    all_to_all x2 -> x0, blocking collectives: 56.5 us -> none  [the longest x1 52.6 us: local(): lax.all_to_all(outgoing.reshape(expert_count, capacity, width), 'sp', spl...]
    all_to_all x1, waiting for transfers between devices: 48.3 us -> 1.06 us  [local(): lax.all_to_all(attn_out, 'tp', split_axis=0, concat_axis=1, tiled=True)]
    all_gather x3 -> x0, blocking collectives: 41.4 us -> none  [the longest x1 36 us: local(): rot_rows = lax.all_gather(paired[1], 'sp', axis=0, tiled=True)]
    all_gather x2 -> x0, waiting for transfers between devices: 33.3 us -> none  [the longest x1 19.3 us: local(): lat_rows = lax.all_gather(paired[0], 'sp', axis=0, tiled=True)]
    dot_general x12 -> x5, matrix products: 46.2 us -> 19.2 us  [the longest x1 9.1 us: local(): jnp.dot(activated, w_down[0], preferred_element_type=jnp.float32)]
    reduce_scatter x1 -> x0, waiting for transfers between devices: 13.5 us -> none  [local(): lax.psum_scatter(lax.optimization_barrier(product.astype(jnp.bfloat16)).a...]
    reduce_sum x3 -> x1, other arithmetic: 7.83 us -> 0.14 us  [local(): shares = jnp.sum(jnp.where(chosen, route_weight[:, :, None], 0.0), axis=1)]
  transfers between devices with their start and end apart: 4 -> 1, of which waited for: 4 -> 1; matrix products, arithmetic and copies ran while one was open for 2% -> 0% of each run, Pallas kernels for 0% -> 0%
where the time goes in v1:
time: 206 us
  Pallas kernels  168 us (82%)
  matrix products  22.2 us (11%)
  local copies, waits for them, and re-layouts  6.54 us (3%)
  other arithmetic  4.1 us (2%)
  starting transfers between devices  3.62 us (2%)
    pallas_call x1, Pallas kernels, dispatch_rows(): pl.pallas_call(functools.partial(dispatch_kernel, n_sp, n_tp), out_shape=...  67.1 us
    pallas_call x1, Pallas kernels, return_rows(): pl.pallas_call(functools.partial(return_kernel, n_sp, n_tp), out_shape=ja...  59 us
    pallas_call x1, Pallas kernels, gather_rows(): pl.pallas_call(functools.partial(gather_kernel, n_sp, n_tp, inner), out_s...  28.6 us
    pallas_call x1, Pallas kernels, attention(): pl.pallas_call(functools.partial(attention_kernel, key_block, latent_widt...  13.2 us
    dot_general x1, matrix products, local(): jnp.dot(activated, w_down[0], preferred_element_type=jnp.float32)  9.1 us
    dot_general x1, matrix products, local(): gate_part = jnp.dot(received, w_gate[0], preferred_element_type=jnp.float32)  4.52 us
  transfers between devices with their start and end apart: 1, of which 1 were waited for; matrix products, arithmetic and copies ran while one was open for 0% of the time, Pallas kernels for 0%

profile of v1, /device:TPU:16, one launch (start us, length us, event | category | flops | bytes accessed | tf_op | source)
XLA Modules:
  0.0 205.7 jit_solution(15627598906878875199)
XLA Ops:
  0.0 0.0 copy-start
  0.0 0.0 copy-start.3
  0.0 0.1 pad.7.clone
  0.1 0.1 pad.3.clone
  0.2 1.0 copy.44
  1.2 1.1 copy.43
  2.3 0.8 copy.45
  3.1 0.2 multiply_cosine_fusion.1
  3.3 0.3 fusion.27
  3.7 1.6 maximum_maximum_fusion.own_ref
  5.2 28.6 %gather_rows.1 = bf16[32,128,384]{2,1,0:T(8,128)(2,1)} custom-call(bf16[128,384]{1,0:T(8,128)(2,1)} %maximum_maximum_fusion.own_ref), custom_call_target="tpu_custom_call" | custom-call | tf_op jit(solution)/shard_map/gather_rows/pallas_call | solution.py:123
  33.8 0.0 copy-done.3
  33.8 0.0 copy-start.5
  33.8 0.0 copy-start.2
  33.8 0.9 copy.47
  34.7 0.9 maximum_bitcast_fusion.query_ref
  35.7 13.2 %attention.1 = bf16[256,512]{1,0:T(8,128)(2,1)} custom-call(s32[1]{0:T(128)} %bitcast.base_ref, bf16[4,256,256]{2,1,0:T(8,128)(2,1)} %maximum_bitcast_fusion.query_ref, bf16[4096,384]{1,0:T(8,128)(2,1)} %bitcast.49, bf16[256,512]{1,0:T(8,128)(2,1)} %key_up_ref.1, bf16[512,256]{1,0:T(8,128)(2,1)} %bitcast.56), custom_call_target="tpu_custom_call" | custom-call | tf_op jit(solution)/shard_map/attention/pallas_call | solution.py:323
  48.9 0.0 copy-start.4
  48.9 1.8 copy.48
  50.7 3.6 %all-to-all-start = ((bf16[2,128,512]{1,2,0:T(8,128)(2,1)}), bf16[2,128,512]{1,2,0:T(8,128)(2,1)S(1)}, u32[]{:S(2)}, u32[]{:S(2)}) async-start(bf16[2,128,512]{1,2,0:T(8,128)(2,1)} %copy.48), calls=%async_computation | async-start | bytes 524288 | tf_op jit(solution)/shard_map/all_to_all | solution.py:387
  54.3 0.0 copy-done.5
  54.3 0.1 copy.49
  54.5 0.1 eq.42
  54.6 0.1 eq.38
  54.7 1.1 all-to-all-done
  55.8 0.0 copy-done.2
  55.8 3.0 %multiply_reduce_fusion = (f32[128]{0:T(128)S(1)}, f32[128,2048]{1,0:T(8,128)S(1)}) fusion(bf16[128,1024]{0,1:T(8,128)(2,1)S(1)} %bitcast.57, bf16[1024,2048]{1,0:T(8,128)(2,1)} %param.21, bf16[128,2048]{1,0:T(8,128)(2,1)S(1)} %copy-done.2), kind=kOutput, calls=%fused_computation.20 | convolution fusion | flops 538443648 | bytes 6029824 | tf_op jit(solution)/shard_map/dot_general | solution.py:388
  58.8 0.6 reduce-window.6
  59.4 0.2 slice_reduce_fusion
  59.7 0.1 fusion.31
  59.8 0.1 sub.18
  59.9 0.1 copy.52
  60.0 0.1 fusion.18
  60.1 0.0 copy-done.4
  60.1 2.1 %convolution_convert_fusion.1 = bf16[512,2048]{1,0:T(8,128)(2,1)} fusion(pred[128,512]{1,0:T(8,128)(4,1)S(1)} %fusion.18, f32[128,2048]{1,0:T(8,128)S(1)} %get-tuple-element.12, f32[2048]{0:T(1024)S(1)} %copy-done.4, f32[128]{0:T(128)S(1)} %add_rsqrt_fusion), kind=kOutput, calls=%fused_computation.1 | convolution fusion | flops 270270464 | bytes 3219968 | tf_op jit(solution)/shard_map/dot_general | solution.py:411
  62.2 0.0 copy-start.7
  62.3 67.1 %dispatch_rows.1 = bf16[2,16,32,2048]{3,2,1,0:T(8,128)(2,1)} custom-call(bf16[16,32,2048]{2,1,0:T(8,128)(2,1)} %bitcast.50), custom_call_target="tpu_custom_call" | custom-call | tf_op jit(solution)/shard_map/dispatch_rows/pallas_call | solution.py:177
  129.4 0.0 copy-done.7
  129.4 4.5 %fusion.8 = f32[1024,256]{1,0:T(8,128)} fusion(bf16[1024,2048]{1,0:T(8,128)(2,1)} %bitcast.51, bf16[1,2048,256]{2,1,0:T(8,128)(2,1)S(1)} %copy-done.7), kind=kOutput, calls=%fused_computation.12 | convolution fusion | flops 1073741824 | bytes 6291456 | tf_op jit(solution)/shard_map/dot_general | solution.py:420
  133.9 0.0 copy-done
  133.9 9.1 %convolution_convert_fusion = bf16[1024,2048]{1,0:T(8,128)(2,1)} fusion(bf16[1024,2048]{1,0:T(8,128)(2,1)} %bitcast.52, bf16[1,256,2048]{2,1,0:T(8,128)(2,1)S(1)} %copy-done, bf16[1,2048,256]{2,1,0:T(8,128)(2,1)} %param.26, f32[1024,256]{1,0:T(8,128)} %fusion.8), kind=kOutput, calls=%fused_computation | convolution fusion | flops 2151153664 | bytes 11534336 | tf_op jit(solution)/shard_map/dot_general | solution.py:423
  143.0 0.0 copy-start.6
  143.0 59.0 %return_rows.1 = bf16[16,32,2048]{2,1,0:T(8,128)(2,1)} custom-call(bf16[2,16,32,2048]{3,2,1,0:T(8,128)(2,1)} %bitcast.53), custom_call_target="tpu_custom_call" | custom-call | tf_op jit(solution)/shard_map/return_rows/pallas_call | solution.py:239
  202.1 0.0 copy-done.6
  202.1 0.0 copy-start.1
  202.1 0.1 select_reduce_fusion
  202.3 2.2 %fusion.21 = f32[128,2048]{1,0:T(8,128)S(1)} fusion(bf16[512,2048]{1,0:T(8,128)(2,1)} %bitcast.47, f32[128,512]{1,0:T(8,128)S(1)} %select_reduce_fusion), kind=kOutput, calls=%fused_computation.31 | convolution fusion | flops 268566528 | bytes 3407872 | tf_op jit(solution)/shard_map/dot_general | solution.py:427
  204.4 0.0 copy-done.1
  204.4 1.3 fusion.3
  (12 shorter events, 0.1 us)
Async XLA Ops:
  0.0 133.9 %copy-start = (bf16[1,256,2048]{2,1,0:T(8,128)(2,1)S(1)}, bf16[1,256,2048]{2,1,0:T(8,128)(2,1)}, u32[]{:S(2)}) copy-start(bf16[1,256,2048]{2,1,0:T(8,128)(2,1)} %param.27) | copy-start | bytes 3145732
  0.0 33.8 %copy-start.3 = (bf16[256,512]{1,0:T(8,128)(2,1)S(1)}, bf16[256,512]{1,0:T(8,128)(2,1)}, u32[]{:S(2)}) copy-start(bf16[256,512]{1,0:T(8,128)(2,1)} %param.20) | copy-start | bytes 786436
  33.8 20.5 %copy-start.5 = (s32[128,2]{0,1:T(2,128)S(1)}, s32[128,2]{0,1:T(2,128)}, u32[]{:S(2)}) copy-start(s32[128,2]{0,1:T(2,128)} %param.23) | copy-start | bytes 3076
  33.8 22.0 %copy-start.2 = (bf16[128,2048]{1,0:T(8,128)(2,1)S(1)}, bf16[128,2048]{1,0:T(8,128)(2,1)}, u32[]{:S(2)}) copy-start(bf16[128,2048]{1,0:T(8,128)(2,1)} %param.14) | copy-start | bytes 1572868
  48.9 11.2 %copy-start.4 = (f32[2048]{0:T(1024)S(1)}, f32[2048]{0:T(1024)}, u32[]{:S(2)}) copy-start(f32[2048]{0:T(1024)} %param.22) | copy-start | bytes 24580
  50.7 5.1 %all-to-all-start = ((bf16[2,128,512]{1,2,0:T(8,128)(2,1)}), bf16[2,128,512]{1,2,0:T(8,128)(2,1)S(1)}, u32[]{:S(2)}, u32[]{:S(2)}) async-start(bf16[2,128,512]{1,2,0:T(8,128)(2,1)} %copy.48), calls=%async_computation | async-start | bytes 524288 | tf_op jit(solution)/shard_map/all_to_all | solution.py:387
  62.2 67.2 %copy-start.7 = (bf16[1,2048,256]{2,1,0:T(8,128)(2,1)S(1)}, bf16[1,2048,256]{2,1,0:T(8,128)(2,1)}, u32[]{:S(2)}) copy-start(bf16[1,2048,256]{2,1,0:T(8,128)(2,1)} %param.25) | copy-start | bytes 3145732
  143.0 59.1 %copy-start.6 = (f32[128,2]{0,1:T(2,128)S(1)}, f32[128,2]{0,1:T(2,128)}, u32[]{:S(2)}) copy-start(f32[128,2]{0,1:T(2,128)} %param.24) | copy-start | bytes 3076
  202.1 2.3 %copy-start.1 = (bf16[16,32,2048]{2,1,0:T(8,128)(2,1)S(1)}, bf16[16,32,2048]{2,1,0:T(8,128)(2,1)}, u32[]{:S(2)}) copy-start(bf16[16,32,2048]{2,1,0:T(8,128)(2,1)} %return_rows.1) | copy-start | bytes 6291460

commit v2 on v1

--- a/solution.py
+++ b/solution.py
@@ -135,124 +135,160 @@
     )(own)
 
 
-def dispatch_kernel(n_sp, n_tp, rows_ref, out_ref, send_sem, recv_sem, local_sem):
+def expert_kernel(
+    n_sp,
+    n_tp,
+    cap,
+    batch,
+    rows_ref,
+    gate_ref,
+    up_ref,
+    down_ref,
+    out_ref,
+    in_ref,
+    part_ref,
+    half_ref,
+    sum_ref,
+    in_send,
+    in_recv,
+    twin_send,
+    twin_recv,
+    back_send,
+    back_recv,
+    local_sem,
+):
     sp, tp = lax.axis_index("sp"), lax.axis_index("tp")
-    peers = [((sp + step) % n_sp, tp) for step in far_first(n_sp)]
-    twins = [(sp, (tp + step) % n_tp) for step in range(1, n_tp)]
-    greet(peers + twins)
+    steps = far_first(n_sp) + [0]
+    twins = [(sp, (tp + hop) % n_tp) for hop in range(1, n_tp)]
+    targets = [((sp + step) % n_sp, tp) for step in steps]
+    origins = [((sp + n_sp - step) % n_sp, tp) for step in steps]
+    greet(targets[:-1] + twins)
     copies = []
 
-    def push(source, core, origin, peer):
+    def span(index):
+        return pl.ds(pl.multiple_of(index * cap, cap), cap)
+
+    keep_in = pltpu.make_async_copy(
+        rows_ref.at[span(sp)], in_ref.at[span((n_sp - 1) * n_tp + tp)], local_sem.at[0]
+    )
+    keep_in.start()
+    for place in range(n_sp - 1):
         copies.append(
             send(
-                source,
-                out_ref.at[core, origin],
-                send_sem.at[len(copies)],
-                recv_sem.at[core * n_sp + origin],
-                peer,
+                rows_ref.at[span(targets[place][0])],
+                in_ref.at[span(place * n_tp + tp)],
+                in_send.at[place],
+                in_recv.at[place * n_tp + tp],
+                targets[place],
             )
         )
 
-    keep = pltpu.make_async_copy(rows_ref.at[sp], out_ref.at[tp, sp], local_sem)
-    keep.start()
-    for peer in peers:
-        push(rows_ref.at[peer[0]], tp, sp, peer)
-    for twin in twins:
-        push(rows_ref.at[sp], tp, sp, twin)
-    for step in reversed(far_first(n_sp)):
-        origin = (sp + step) % n_sp
-        arrived(out_ref.at[tp, origin], recv_sem.at[tp * n_sp + origin])
-        for twin in twins:
-            push(out_ref.at[tp, origin], tp, origin, twin)
-    for twin in twins:
-        for origin in range(n_sp):
-            arrived(out_ref.at[twin[1], origin], recv_sem.at[twin[1] * n_sp + origin])
-    keep.wait()
-    for copy in copies:
-        copy.wait_send()
-
-
-def dispatch_rows(rows, n_sp, n_tp):
-    sends = n_sp - 1 + n_sp * (n_tp - 1)
-    return pl.pallas_call(
-        functools.partial(dispatch_kernel, n_sp, n_tp),
-        out_shape=jax.ShapeDtypeStruct((n_tp,) + rows.shape, rows.dtype),
-        in_specs=[VMEM],
-        out_specs=VMEM,
-        scratch_shapes=[
-            pltpu.SemaphoreType.DMA((sends,)),
-            pltpu.SemaphoreType.DMA((n_sp * n_tp,)),
-            pltpu.SemaphoreType.DMA,
-        ],
-        compiler_params=pltpu.CompilerParams(collective_id=1, has_side_effects=True),
-        name="dispatch_rows",
-    )(rows)
-
-
-def return_kernel(
-    n_sp, n_tp, part_ref, out_ref, half_ref, sum_ref, twin_send, twin_recv, send_sem, recv_sem, local_sem
-):
-    sp, tp = lax.axis_index("sp"), lax.axis_index("tp")
-    order = far_first(n_sp)
-    peers = [((sp + step) % n_sp, tp) for step in order]
-    twins = [(sp, (tp + step) % n_tp) for step in range(1, n_tp)]
-    greet(peers + twins)
-    copies = []
-    for target in [peer[0] for peer in peers] + [sp]:
-        for step, twin in enumerate(twins):
-            slot = step * n_sp + target
+    def forward(place):
+        block = place * n_tp + tp
+        if place < n_sp - 1:
+            arrived(in_ref.at[span(block)], in_recv.at[block])
+        for hop, twin in enumerate(twins):
             copies.append(
                 send(
-                    part_ref.at[twin[1], target],
-                    half_ref.at[step, target],
-                    twin_send.at[slot],
-                    twin_recv.at[slot],
+                    rows_ref.at[span(sp)] if place == n_sp - 1 else in_ref.at[span(block)],
+                    in_ref.at[span(block)],
+                    in_send.at[n_sp - 1 + hop * n_sp + place],
+                    in_recv.at[block],
                     twin,
                 )
             )
 
-    def total(target):
-        value = part_ref[tp, target].astype(jnp.float32)
-        for step in range(n_tp - 1):
-            arrived(half_ref.at[step, target], twin_recv.at[step * n_sp + target])
-            value = value + half_ref[step, target].astype(jnp.float32)
-        sum_ref[target] = value.astype(sum_ref.dtype)
-
-    for number, peer in enumerate(peers):
-        total(peer[0])
-        copies.append(
-            send(sum_ref.at[peer[0]], out_ref.at[sp], send_sem.at[number], recv_sem.at[sp], peer)
-        )
-    total(sp)
-    keep = pltpu.make_async_copy(sum_ref.at[sp], out_ref.at[sp], local_sem)
-    keep.start()
-    for step in reversed(order):
-        origin = (sp + step) % n_sp
-        arrived(out_ref.at[origin], recv_sem.at[origin])
-    keep.wait()
+    def compute(places):
+        for place in places:
+            for twin in twins:
+                block = place * n_tp + twin[1]
+                arrived(in_ref.at[span(block)], in_recv.at[block])
+        if places[-1] == n_sp - 1:
+            keep_in.wait()
+        whole = slice(places[0] * n_tp * cap, (places[-1] + 1) * n_tp * cap)
+        rows = in_ref[whole, :]
+        gate = jnp.dot(rows, gate_ref[...], preferred_element_type=jnp.float32)
+        up = jnp.dot(rows, up_ref[...], preferred_element_type=jnp.float32)
+        activated = (gate / (1.0 + jnp.exp(-gate)) * up).astype(jnp.bfloat16)
+        part_ref[whole, :] = jnp.dot(
+            activated, down_ref[...], preferred_element_type=jnp.float32
+        ).astype(jnp.bfloat16)
+        for place in places:
+            for hop, twin in enumerate(twins):
+                slot = hop * n_sp + place
+                copies.append(
+                    send(
+                        part_ref.at[span(place * n_tp + twin[1])],
+                        half_ref.at[span(slot)],
+                        twin_send.at[slot],
+                        twin_recv.at[slot],
+                        twin,
+                    )
+                )
+
+    def finish(places):
+        for place in places:
+            value = part_ref[span(place * n_tp + tp), :].astype(jnp.float32)
+            for hop in range(n_tp - 1):
+                slot = hop * n_sp + place
+                arrived(half_ref.at[span(slot)], twin_recv.at[slot])
+                value = value + half_ref[span(slot), :].astype(jnp.float32)
+            if place == n_sp - 1:
+                out_ref[span(sp), :] = value.astype(out_ref.dtype)
+            else:
+                sum_ref[span(place), :] = value.astype(sum_ref.dtype)
+                copies.append(
+                    send(
+                        sum_ref.at[span(place)],
+                        out_ref.at[span(sp)],
+                        back_send.at[place],
+                        back_recv.at[sp],
+                        origins[place],
+                    )
+                )
+
+    batches = [list(range(n_sp))[first : first + batch] for first in range(0, n_sp, batch)]
+    for place in batches[0]:
+        forward(place)
+    for number, places in enumerate(batches):
+        compute(places)
+        if number > 0:
+            finish(batches[number - 1])
+        if number + 1 < len(batches):
+            for place in batches[number + 1]:
+                forward(place)
+    finish(batches[-1])
+    for target in targets[:-1]:
+        arrived(out_ref.at[span(target[0])], back_recv.at[target[0]])
     for copy in copies:
         copy.wait_send()
 
 
-def return_rows(parts, n_sp, n_tp):
-    shape = parts.shape[1:]
+def expert_rows(rows, gate, up, down, n_sp, n_tp):
+    cap = rows.shape[0] // n_sp
+    width = rows.shape[1]
+    dma = pltpu.SemaphoreType.DMA
     return pl.pallas_call(
-        functools.partial(return_kernel, n_sp, n_tp),
-        out_shape=jax.ShapeDtypeStruct(shape, parts.dtype),
-        in_specs=[VMEM],
+        functools.partial(expert_kernel, n_sp, n_tp, cap, math.gcd(n_sp, 256 // (n_tp * cap))),
+        out_shape=jax.ShapeDtypeStruct(rows.shape, rows.dtype),
+        in_specs=[VMEM] * 4,
         out_specs=VMEM,
         scratch_shapes=[
-            pltpu.VMEM((n_tp - 1,) + shape, parts.dtype),
-            pltpu.VMEM(shape, parts.dtype),
-            pltpu.SemaphoreType.DMA(((n_tp - 1) * n_sp,)),
-            pltpu.SemaphoreType.DMA(((n_tp - 1) * n_sp,)),
-            pltpu.SemaphoreType.DMA((n_sp - 1,)),
-            pltpu.SemaphoreType.DMA((n_sp,)),
-            pltpu.SemaphoreType.DMA,
+            pltpu.VMEM((n_sp * n_tp * cap, width), rows.dtype),
+            pltpu.VMEM((n_sp * n_tp * cap, width), rows.dtype),
+            pltpu.VMEM((n_sp * (n_tp - 1) * cap, width), rows.dtype),
+            pltpu.VMEM(rows.shape, rows.dtype),
+            dma((n_sp - 1 + n_sp * (n_tp - 1),)),
+            dma((n_sp * n_tp,)),
+            dma((n_sp * (n_tp - 1),)),
+            dma((n_sp * (n_tp - 1),)),
+            dma((n_sp - 1,)),
+            dma((n_sp,)),
+            dma((1,)),
         ],
-        compiler_params=pltpu.CompilerParams(collective_id=2, has_side_effects=True),
-        name="return_rows",
-    )(parts)
+        compiler_params=pltpu.CompilerParams(collective_id=1, has_side_effects=True),
+        name="expert_rows",
+    )(rows, gate, up, down)
 
 
 NT = (((1,), (1,)), ((), ()))
@@ -395,6 +431,7 @@
     normed = (normed * norm_gain[None, :]).astype(jnp.bfloat16)
     expert_count = lax.axis_size("sp")
     capacity = max(2, 2 * (row_count * tp_count) // expert_count)
+    capacity = -(-capacity // 16) * 16
     top_count = routes.shape[1]
     width = normed.shape[1]
     flat_expert = routes.reshape(-1)
@@ -414,16 +451,7 @@
     shares = jnp.sum(jnp.where(chosen, route_weight[:, :, None], 0.0), axis=1)
     share_high = lax.reduce_precision(shares, 8, 7)
     share_low = shares - share_high
-    received = dispatch_rows(
-        outgoing.reshape(expert_count, capacity, width), sp_count, tp_count
-    ).reshape(tp_count * slot_count, width)
-    gate_part = jnp.dot(received, w_gate[0], preferred_element_type=jnp.float32)
-    up_part = jnp.dot(received, w_up[0], preferred_element_type=jnp.float32)
-    activated = (jax.nn.silu(gate_part) * up_part).astype(jnp.bfloat16)
-    product = jnp.dot(activated, w_down[0], preferred_element_type=jnp.float32).astype(jnp.bfloat16)
-    back_rows = return_rows(
-        product.reshape(tp_count, expert_count, capacity, width), sp_count, tp_count
-    ).reshape(slot_count, width)
+    back_rows = expert_rows(outgoing, w_gate[0], w_up[0], w_down[0], sp_count, tp_count)
     combined = jnp.dot(
         share_high.astype(jnp.bfloat16), back_rows, preferred_element_type=jnp.float32
     ) + jnp.dot(share_low.astype(jnp.bfloat16), back_rows, preferred_element_type=jnp.float32)

time: 206 us -> 178 us (0.86)
  Pallas kernels: 168 us -> 154 us
  matrix products: 22.2 us -> 8.65 us
    pallas_call x2 -> x1, Pallas kernels: 126 us -> 112 us  [expert_rows(): pl.pallas_call(functools.partial(expert_kernel, n_sp, n_tp, cap, math.gcd...]
    dot_general x2 -> x0, matrix products: 13.6 us -> none  [the longest x1 9.1 us: local(): jnp.dot(activated, w_down[0], preferred_element_type=jnp.float32)]
where the time goes in v2:
time: 178 us
  Pallas kernels  154 us (87%)
  matrix products  8.65 us (5%)
  local copies, waits for them, and re-layouts  6.58 us (4%)
  other arithmetic  4.1 us (2%)
  starting transfers between devices  3.62 us (2%)
    pallas_call x1, Pallas kernels, expert_rows(): pl.pallas_call(functools.partial(expert_kernel, n_sp, n_tp, cap, math.gcd...  112 us
    pallas_call x1, Pallas kernels, gather_rows(): pl.pallas_call(functools.partial(gather_kernel, n_sp, n_tp, inner), out_s...  28.6 us
    pallas_call x1, Pallas kernels, attention(): pl.pallas_call(functools.partial(attention_kernel, key_block, latent_widt...  13.3 us
    all_to_all x1, starting transfers between devices, local(): lax.all_to_all(attn_out, 'tp', split_axis=0, concat_axis=1, tiled=True)  3.62 us
  transfers between devices with their start and end apart: 1, of which 1 were waited for; matrix products, arithmetic and copies ran while one was open for 0% of the time, Pallas kernels for 0%

profile of v2, /device:TPU:16, one launch (start us, length us, event | category | flops | bytes accessed | tf_op | source)
XLA Modules:
  0.0 177.8 jit_solution(3512367169445792658)
XLA Ops:
  0.0 0.1 pad.7.clone
  0.1 0.1 pad.3.clone
  0.2 1.0 copy.44
  1.2 0.0 copy-start.2
  1.2 1.1 copy.43
  2.3 0.8 copy.45
  3.2 0.2 multiply_cosine_fusion.1
  3.4 0.3 fusion.15
  3.7 1.6 maximum_maximum_fusion.own_ref
  5.3 28.6 %gather_rows.1 = bf16[32,128,384]{2,1,0:T(8,128)(2,1)} custom-call(bf16[128,384]{1,0:T(8,128)(2,1)} %maximum_maximum_fusion.own_ref), custom_call_target="tpu_custom_call" | custom-call | tf_op jit(solution)/shard_map/gather_rows/pallas_call | solution.py:123
  33.9 0.0 copy-done.2
  33.9 0.9 copy.47
  34.8 0.9 maximum_bitcast_fusion.query_ref
  35.7 0.0 copy-start.4
  35.7 0.0 copy-start.1
  35.7 13.3 %attention.1 = bf16[256,512]{1,0:T(8,128)(2,1)} custom-call(s32[1]{0:T(128)} %bitcast.base_ref, bf16[4,256,256]{2,1,0:T(8,128)(2,1)} %maximum_bitcast_fusion.query_ref, bf16[4096,384]{1,0:T(8,128)(2,1)} %bitcast.34, bf16[256,512]{1,0:T(8,128)(2,1)} %key_up_ref.1, bf16[512,256]{1,0:T(8,128)(2,1)} %bitcast.40), custom_call_target="tpu_custom_call" | custom-call | tf_op jit(solution)/shard_map/attention/pallas_call | solution.py:359
  49.0 1.8 %copy.48 = bf16[2,128,512]{1,2,0:T(8,128)(2,1)} copy(bf16[2,128,512]{2,1,0:T(8,128)(2,1)} %bitcast.42) | data formatting | bytes 524288 | tf_op jit(solution)/shard_map/all_to_all | solution.py:423
  50.8 3.6 %all-to-all-start = ((bf16[2,128,512]{1,2,0:T(8,128)(2,1)}), bf16[2,128,512]{1,2,0:T(8,128)(2,1)S(1)}, u32[]{:S(2)}, u32[]{:S(2)}) async-start(bf16[2,128,512]{1,2,0:T(8,128)(2,1)} %copy.48), calls=%async_computation | async-start | bytes 524288 | tf_op jit(solution)/shard_map/all_to_all | solution.py:423
  54.4 0.0 copy-done.4
  54.4 0.1 copy.49
  54.5 0.1 eq.42
  54.7 0.1 eq.38
  54.8 1.1 all-to-all-done
  55.9 0.0 copy-done.1
  55.9 0.0 copy-start.5
  55.9 0.0 copy-start.3
  55.9 3.0 %multiply_reduce_fusion = (f32[128]{0:T(128)S(1)}, f32[128,2048]{1,0:T(8,128)S(1)}) fusion(bf16[128,1024]{0,1:T(8,128)(2,1)S(1)} %bitcast.41, bf16[1024,2048]{1,0:T(8,128)(2,1)} %param.21, bf16[128,2048]{1,0:T(8,128)(2,1)S(1)} %copy-done.1), kind=kOutput, calls=%fused_computation.8 | convolution fusion | flops 538443648 | bytes 6029824 | tf_op jit(solution)/shard_map/dot_general | solution.py:424
  58.9 0.6 reduce-window.6
  59.5 0.2 slice_reduce_fusion
  59.8 0.1 fusion.19
  59.8 0.1 sub.18
  60.0 0.1 copy.52
  60.1 0.1 fusion.6
  60.2 0.0 copy-done.5
  60.2 0.1 select_reduce_fusion
  60.4 0.0 copy-done.3
  60.4 2.1 %convolution_convert_fusion.rows_ref = bf16[512,2048]{1,0:T(8,128)(2,1)} fusion(pred[128,512]{1,0:T(8,128)(4,1)S(1)} %fusion.6, f32[128,2048]{1,0:T(8,128)S(1)} %get-tuple-element.12, f32[2048]{0:T(1024)S(1)} %copy-done.3, f32[128]{0:T(128)S(1)} %add_rsqrt_fusion), kind=kOutput, calls=%fused_computation | convolution fusion | flops 270270464 | bytes 3219968 | tf_op jit(solution)/shard_map/dot_general | solution.py:448
  62.5 111.8 %expert_rows.1 = bf16[512,2048]{1,0:T(8,128)(2,1)} custom-call(bf16[512,2048]{1,0:T(8,128)(2,1)} %convolution_convert_fusion.rows_ref, bf16[2048,256]{1,0:T(8,128)(2,1)} %bitcast.35, bf16[2048,256]{1,0:T(8,128)(2,1)} %bitcast.36, bf16[256,2048]{1,0:T(8,128)(2,1)} %bitcast.37), custom_call_target="tpu_custom_call" | custom-call | tf_op jit(solution)/shard_map/expert_rows/pallas_call | solution.py:271
  174.3 0.0 copy-start
  174.3 2.2 %fusion.9 = f32[128,2048]{1,0:T(8,128)S(1)} fusion(bf16[512,2048]{1,0:T(8,128)(2,1)} %expert_rows.1, f32[128,512]{1,0:T(8,128)S(1)} %select_reduce_fusion), kind=kOutput, calls=%fused_computation.18 | convolution fusion | flops 268566528 | bytes 3407872 | tf_op jit(solution)/shard_map/dot_general | solution.py:455
  176.5 0.0 copy-done
  176.5 1.3 fusion.3
  (12 shorter events, 0.1 us)
Async XLA Ops:
  1.2 32.7 %copy-start.2 = (bf16[256,512]{1,0:T(8,128)(2,1)S(1)}, bf16[256,512]{1,0:T(8,128)(2,1)}, u32[]{:S(2)}) copy-start(bf16[256,512]{1,0:T(8,128)(2,1)} %param.20) | copy-start | bytes 786436
  35.7 18.7 %copy-start.4 = (s32[128,2]{0,1:T(2,128)S(1)}, s32[128,2]{0,1:T(2,128)}, u32[]{:S(2)}) copy-start(s32[128,2]{0,1:T(2,128)} %param.23) | copy-start | bytes 3076
  35.7 20.2 %copy-start.1 = (bf16[128,2048]{1,0:T(8,128)(2,1)S(1)}, bf16[128,2048]{1,0:T(8,128)(2,1)}, u32[]{:S(2)}) copy-start(bf16[128,2048]{1,0:T(8,128)(2,1)} %param.14) | copy-start | bytes 1572868
  50.8 5.1 %all-to-all-start = ((bf16[2,128,512]{1,2,0:T(8,128)(2,1)}), bf16[2,128,512]{1,2,0:T(8,128)(2,1)S(1)}, u32[]{:S(2)}, u32[]{:S(2)}) async-start(bf16[2,128,512]{1,2,0:T(8,128)(2,1)} %copy.48), calls=%async_computation | async-start | bytes 524288 | tf_op jit(solution)/shard_map/all_to_all | solution.py:423
  55.9 4.3 %copy-start.5 = (f32[128,2]{0,1:T(2,128)S(1)}, f32[128,2]{0,1:T(2,128)}, u32[]{:S(2)}) copy-start(f32[128,2]{0,1:T(2,128)} %param.24) | copy-start | bytes 3076
  55.9 4.5 %copy-start.3 = (f32[2048]{0:T(1024)S(1)}, f32[2048]{0:T(1024)}, u32[]{:S(2)}) copy-start(f32[2048]{0:T(1024)} %param.22) | copy-start | bytes 24580
  174.3 2.2 %copy-start = (bf16[512,2048]{1,0:T(8,128)(2,1)S(1)}, bf16[512,2048]{1,0:T(8,128)(2,1)}, u32[]{:S(2)}) copy-start(bf16[512,2048]{1,0:T(8,128)(2,1)} %expert_rows.1) | copy-start | bytes 6291460

commit v3 on v2

--- a/solution.py
+++ b/solution.py
@@ -289,6 +289,44 @@
         compiler_params=pltpu.CompilerParams(collective_id=1, has_side_effects=True),
         name="expert_rows",
     )(rows, gate, up, down)
+
+
+def heads_kernel(n_tp, own_ref, out_ref, send_sem, recv_sem, local_sem):
+    sp, tp = lax.axis_index("sp"), lax.axis_index("tp")
+    twins = [(sp, (tp + hop) % n_tp) for hop in range(1, n_tp)]
+    greet(twins)
+    rows = out_ref.shape[1]
+
+    def part(core):
+        return own_ref.at[pl.ds(pl.multiple_of(core * rows, rows), rows)]
+
+    copies = [
+        send(part(twin[1]), out_ref.at[tp], send_sem.at[hop], recv_sem.at[tp], twin)
+        for hop, twin in enumerate(twins)
+    ]
+    keep = pltpu.make_async_copy(part(tp), out_ref.at[tp], local_sem)
+    keep.start()
+    for twin in twins:
+        arrived(out_ref.at[twin[1]], recv_sem.at[twin[1]])
+    keep.wait()
+    for copy in copies:
+        copy.wait_send()
+
+
+def swap_heads(own, n_tp):
+    return pl.pallas_call(
+        functools.partial(heads_kernel, n_tp),
+        out_shape=jax.ShapeDtypeStruct((n_tp, own.shape[0] // n_tp, own.shape[1]), own.dtype),
+        in_specs=[VMEM],
+        out_specs=VMEM,
+        scratch_shapes=[
+            pltpu.SemaphoreType.DMA((n_tp - 1,)),
+            pltpu.SemaphoreType.DMA((n_tp,)),
+            pltpu.SemaphoreType.DMA,
+        ],
+        compiler_params=pltpu.CompilerParams(collective_id=2, has_side_effects=True),
+        name="swap_heads",
+    )(own)
 
 
 NT = (((1,), (1,)), ((), ()))
@@ -420,8 +458,13 @@
         key_block,
         latent.shape[1],
     )
-    all_heads = lax.all_to_all(attn_out, "tp", split_axis=0, concat_axis=1, tiled=True)
-    projected = jnp.dot(all_heads, out_proj, preferred_element_type=jnp.float32)
+    all_heads = swap_heads(attn_out, tp_count)
+    proj_parts = out_proj.reshape(tp_count, attn_out.shape[1], out_proj.shape[1])
+    projected = jnp.dot(all_heads[0], proj_parts[0], preferred_element_type=jnp.float32)
+    for core in range(1, tp_count):
+        projected = projected + jnp.dot(
+            all_heads[core], proj_parts[core], preferred_element_type=jnp.float32
+        )
     hidden_wide = residual.astype(jnp.float32) + projected
     hidden = hidden_wide.astype(jnp.bfloat16)
     hidden_wide = hidden.astype(jnp.float32)

time: 178 us -> 176 us (0.989)
  Pallas kernels: 154 us -> 158 us
  starting transfers between devices: 3.62 us -> 0 us
  local copies, waits for them, and re-layouts: 6.58 us -> 4.03 us
    all_to_all x1 -> x0, starting transfers between devices: 3.62 us -> none  [local(): lax.all_to_all(attn_out, 'tp', split_axis=0, concat_axis=1, tiled=True)]
    pallas_call x0 -> x1, Pallas kernels: none -> 3.16 us  [swap_heads(): pl.pallas_call(functools.partial(heads_kernel, n_tp), out_shape=jax.Shape...]
    all_to_all x1 -> x0, local copies, waits for them, and re-layouts: 1.79 us -> none  [local(): lax.all_to_all(attn_out, 'tp', split_axis=0, concat_axis=1, tiled=True)]
    dot_general x1 -> x2, matrix products: 3.03 us -> 4.43 us  [the longest x1 2.27 us: local(): jnp.dot(all_heads[core], proj_parts[core], preferred_element_type=jnp.flo...]
  transfers between devices with their start and end apart: 1 -> 0, of which waited for: 1 -> 0; matrix products, arithmetic and copies ran while one was open for 0% -> 0% of each run, Pallas kernels for 0% -> 0%
where the time goes in v3:
time: 176 us; the launch traced here: 175 us
  Pallas kernels  158 us (90%)
  matrix products  10 us (6%)
  local copies, waits for them, and re-layouts  4.03 us (2%)
  other arithmetic  3.26 us (2%)
    pallas_call x1, Pallas kernels, expert_rows(): pl.pallas_call(functools.partial(expert_kernel, n_sp, n_tp, cap, math.gcd...  113 us
    pallas_call x1, Pallas kernels, gather_rows(): pl.pallas_call(functools.partial(gather_kernel, n_sp, n_tp, inner), out_s...  28.6 us
    pallas_call x1, Pallas kernels, attention(): pl.pallas_call(functools.partial(attention_kernel, key_block, latent_widt...  13.4 us

profile of v3, /device:TPU:16, one launch (start us, length us, event | category | flops | bytes accessed | tf_op | source)
XLA Modules:
  0.0 175.2 jit_solution(7350379490422024057)
XLA Ops:
  0.0 0.0 copy-start.5
  0.0 0.0 copy-start.4
  0.0 0.2 multiply_cosine_fusion.1
  0.2 1.0 copy.42
  1.3 0.1 pad.7.clone
  1.4 1.1 copy.41
  2.5 0.9 maximum_bitcast_fusion.query_ref
  3.4 0.0 copy-start.3
  3.4 0.0 copy-done.5
  3.4 0.1 copy.43
  3.5 0.3 fusion.23
  3.9 0.1 pad.3.clone
  3.9 0.0 copy-done.4
  3.9 0.7 maximum_maximum_fusion.own_ref
  4.7 28.6 %gather_rows.1 = bf16[32,128,384]{2,1,0:T(8,128)(2,1)} custom-call(bf16[128,384]{1,0:T(8,128)(2,1)} %maximum_maximum_fusion.own_ref), custom_call_target="tpu_custom_call" | custom-call | tf_op jit(solution)/shard_map/gather_rows/pallas_call | solution.py:123
  33.2 0.0 copy-done.3
  33.2 0.8 copy.45
  34.1 13.4 %attention.1.own_ref = bf16[256,512]{1,0:T(8,128)(2,1)} custom-call(s32[1]{0:T(128)} %bitcast.base_ref, bf16[4,256,256]{2,1,0:T(8,128)(2,1)} %maximum_bitcast_fusion.query_ref, bf16[4096,384]{1,0:T(8,128)(2,1)} %bitcast.36, bf16[256,512]{1,0:T(8,128)(2,1)} %key_up_ref.1, bf16[512,256]{1,0:T(8,128)(2,1)} %bitcast.42), custom_call_target="tpu_custom_call" | custom-call | tf_op jit(solution)/shard_map/attention/pallas_call | solution.py:397
  47.5 0.0 copy-start.2
  47.5 3.2 %swap_heads.1 = bf16[2,128,512]{2,1,0:T(8,128)(2,1)} custom-call(bf16[256,512]{1,0:T(8,128)(2,1)} %attention.1.own_ref), custom_call_target="tpu_custom_call" | custom-call | tf_op jit(solution)/shard_map/swap_heads/pallas_call | solution.py:317
  50.7 0.0 copy-start.1
  50.7 2.2 %fusion.6 = f32[128,2048]{1,0:T(8,128)S(1)} fusion(bf16[1024,2048]{1,0:T(8,128)(2,1)} %param.21, bf16[2,128,512]{2,1,0:T(8,128)(2,1)} %swap_heads.1), kind=kOutput, calls=%fused_computation.9 | convolution fusion | flops 268435456 | bytes 3276800 | tf_op jit(solution)/shard_map/dot_general | solution.py:463
  52.8 0.0 copy-done.2
  52.8 0.0 copy-done.1
  52.9 0.0 copy-start.7
  52.9 0.0 copy-start.6
  52.9 2.3 %multiply_reduce_fusion = (f32[128]{0:T(128)S(1)}, f32[128,2048]{1,0:T(8,128)S(1)}) fusion(f32[128,2048]{1,0:T(8,128)S(1)} %fusion.6, bf16[1024,2048]{1,0:T(8,128)(2,1)} %param.21, bf16[2,128,512]{2,1,0:T(8,128)(2,1)S(1)} %copy-done.1, bf16[128,2048]{1,0:T(8,128)(2,1)S(1)} %copy-done.2), kind=kOutput, calls=%fused_computation.12 | convolution fusion | flops 270270336 | bytes 4850176 | tf_op jit(solution)/shard_map/dot_general | solution.py:465
  55.2 0.0 copy-done.7
  55.2 0.1 copy.46
  55.3 0.1 eq.42
  55.4 0.6 reduce-window.6
  56.0 0.2 slice_reduce_fusion
  56.3 0.1 eq.38
  56.4 0.1 fusion.27
  56.5 0.1 sub.18
  56.6 0.1 copy.49
  56.7 0.1 fusion.10
  56.9 0.0 copy-done.6
  56.9 2.1 %convolution_convert_fusion.rows_ref = bf16[512,2048]{1,0:T(8,128)(2,1)} fusion(pred[128,512]{1,0:T(8,128)(4,1)S(1)} %fusion.10, f32[128,2048]{1,0:T(8,128)S(1)} %get-tuple-element.12, f32[2048]{0:T(1024)S(1)} %copy-done.6, f32[128]{0:T(128)S(1)} %add_rsqrt_fusion), kind=kOutput, calls=%fused_computation | convolution fusion | flops 270270464 | bytes 3219968 | tf_op jit(solution)/shard_map/dot_general | solution.py:491
  59.0 0.0 copy-start.8
  59.0 112.6 %expert_rows.1 = bf16[512,2048]{1,0:T(8,128)(2,1)} custom-call(bf16[512,2048]{1,0:T(8,128)(2,1)} %convolution_convert_fusion.rows_ref, bf16[2048,256]{1,0:T(8,128)(2,1)} %bitcast.37, bf16[2048,256]{1,0:T(8,128)(2,1)} %bitcast.38, bf16[256,2048]{1,0:T(8,128)(2,1)} %bitcast.39), custom_call_target="tpu_custom_call" | custom-call | tf_op jit(solution)/shard_map/expert_rows/pallas_call | solution.py:271
  171.6 0.0 copy-done.8
  171.6 0.0 copy-start
  171.6 0.1 select_reduce_fusion
  171.8 2.2 %fusion.13 = f32[128,2048]{1,0:T(8,128)S(1)} fusion(bf16[512,2048]{1,0:T(8,128)(2,1)} %expert_rows.1, f32[128,512]{1,0:T(8,128)S(1)} %select_reduce_fusion), kind=kOutput, calls=%fused_computation.22 | convolution fusion | flops 268566528 | bytes 3407872 | tf_op jit(solution)/shard_map/dot_general | solution.py:498
  173.9 0.0 copy-done
  173.9 1.3 fusion.4
  (12 shorter events, 0.1 us)
Async XLA Ops:
  0.0 3.4 %copy-start.5 = (bf16[128,64]{0,1:T(8,128)(2,1)S(1)}, bf16[128,64]{0,1:T(8,128)(2,1)}, u32[]{:S(2)}) copy-start(bf16[128,64]{0,1:T(8,128)(2,1)} %param.18) | copy-start | bytes 49156
  0.0 3.9 %copy-start.4 = (bf16[128,256]{1,0:T(8,128)(2,1)S(1)}, bf16[128,256]{1,0:T(8,128)(2,1)}, u32[]{:S(2)}) copy-start(bf16[128,256]{1,0:T(8,128)(2,1)} %param.17) | copy-start | bytes 196612
  3.4 29.8 %copy-start.3 = (bf16[256,512]{1,0:T(8,128)(2,1)S(1)}, bf16[256,512]{1,0:T(8,128)(2,1)}, u32[]{:S(2)}) copy-start(bf16[256,512]{1,0:T(8,128)(2,1)} %param.20) | copy-start | bytes 786436
  47.5 5.3 %copy-start.2 = (bf16[128,2048]{1,0:T(8,128)(2,1)S(1)}, bf16[128,2048]{1,0:T(8,128)(2,1)}, u32[]{:S(2)}) copy-start(bf16[128,2048]{1,0:T(8,128)(2,1)} %param.14) | copy-start | bytes 1572868
  50.7 2.2 %copy-start.1 = (bf16[2,128,512]{2,1,0:T(8,128)(2,1)S(1)}, bf16[2,128,512]{2,1,0:T(8,128)(2,1)}, u32[]{:S(2)}) copy-start(bf16[2,128,512]{2,1,0:T(8,128)(2,1)} %swap_heads.1) | copy-start | bytes 786436
  52.9 2.3 %copy-start.7 = (s32[128,2]{0,1:T(2,128)S(1)}, s32[128,2]{0,1:T(2,128)}, u32[]{:S(2)}) copy-start(s32[128,2]{0,1:T(2,128)} %param.23) | copy-start | bytes 3076
  52.9 4.0 %copy-start.6 = (f32[2048]{0:T(1024)S(1)}, f32[2048]{0:T(1024)}, u32[]{:S(2)}) copy-start(f32[2048]{0:T(1024)} %param.22) | copy-start | bytes 24580
  59.0 112.6 %copy-start.8 = (f32[128,2]{0,1:T(2,128)S(1)}, f32[128,2]{0,1:T(2,128)}, u32[]{:S(2)}) copy-start(f32[128,2]{0,1:T(2,128)} %param.24) | copy-start | bytes 3076
  171.6 2.3 %copy-start = (bf16[512,2048]{1,0:T(8,128)(2,1)S(1)}, bf16[512,2048]{1,0:T(8,128)(2,1)}, u32[]{:S(2)}) copy-start(bf16[512,2048]{1,0:T(8,128)(2,1)} %expert_rows.1) | copy-start | bytes 6291460
